TPU v7x, 128 devices: a whole 4x4x4 slice. The times are simulated.
128 devices in a mesh: sp: 32 (over y, x, core), tp: 4 (over z).
Axes of the slice: x: 4, y: 4, z: 4, core: 2. Of those that a mesh axis runs over, the one named last changes fastest.
Arguments:
- block_input: bfloat16 [4096, 1024], P('sp'), may hold values from -6 to 6
- w_query: bfloat16 [1024, 1024], P(None, 'tp'), may hold values from -0.1875 to 0.1875
- w_forget_fwd: bfloat16 [1024, 1024], P(None, 'tp'), may hold values from -0.1875 to 0.1875
- w_forget_bwd: bfloat16 [1024, 1024], P(None, 'tp'), may hold values from -0.1875 to 0.1875
- w_value: bfloat16 [1024, 1024], P(None, 'tp'), may hold values from -0.1875 to 0.1875
- floor_rate: float32 [2, 1024], P(None, 'tp'), may hold values from 0.2 to 6
- gain: float32 [128], replicated, may hold values from 0.1 to 1.9
- cotangent: bfloat16 [4096, 1024], P('sp', 'tp'), may hold values from -6 to 6
Outputs:
- grad_input: bfloat16 [4096, 1024], P(('sp', 'tp'))
- grad_query_weight: float32 [1024, 1024], P('sp', 'tp')
- grad_floor: float32 [2, 1024], P(None, 'tp')
All inputs are finite; a program needn't handle non-finite values.
Results may differ from a plain program's by a relative error of at most 0.0045.
Values sent between devices are 32-bit elements.
No kernel may reach another device: no remote copies, remote signals or barrier semaphores. Data moves between devices by JAX's collectives and lax.ppermute only.
A program may use at most 64 MiB of HBM per device.

v0:
```python
from functools import partial

import jax
import jax.numpy as jnp
from jax import lax
from jax.sharding import Mesh
from jax.sharding import PartitionSpec as P

KDIM = 128
SP = ("sp_0", "sp_1", "sp_2")
SP_TP = ("sp_0", "sp_1", "sp_2", "tp")


FINEST_ROUNDING = lax.Precision.HIGHEST
NORM_EPS = 1e-06


def neutral_like(array, identity):
    return jax.tree.map(
        lambda part, zero: jnp.zeros_like(part) + jnp.asarray(zero, part.dtype), array, identity
    )


def entering(array, axes, combine, identity, reverse):
    before = start = neutral_like(array, identity)
    subtotal = array
    for axis in reversed(axes):
        length, position = lax.axis_size(axis), lax.axis_index(axis)
        pieces = jax.tree.map(lambda part: lax.all_gather(part, axis), subtotal)
        inside, subtotal = start, start
        for k in reversed(range(length)) if reverse else range(length):
            passed = k > position if reverse else k < position
            subtotal = combine(subtotal, jax.tree.map(lambda part: part[k], pieces))
            inside = jax.tree.map(lambda new, old: jnp.where(passed, new, old), subtotal, inside)
        before = combine(inside, before)
    return before


def summed_rows(contribution, width, axis):
    whole = contribution(jnp.int32(0), width * lax.axis_size(axis))
    return lax.psum_scatter(whole, axis, scatter_dimension=0, tiled=True)


def one_axis_at_a_time(array, axes):
    for axis in axes:
        array = lax.psum(array, axis)
    return array


def gate_maps(raw_gate, floor_rates, seq_total):
    step_rate = floor_rates / seq_total
    opening = -jnp.expm1(-step_rate)
    log_forget = jnp.logaddexp(-step_rate, jnp.log(opening) + jax.nn.log_sigmoid(raw_gate))
    return (opening * jax.nn.sigmoid(-raw_gate), log_forget)


def span_output(queries, key_gate, log_forget, payload_entries, arriving_signal):
    cumul = jnp.cumsum(log_forget, axis=0)
    faded_asking_vector = queries * jnp.exp(cumul)
    k_dec = key_gate * jnp.exp(-cumul)
    tok_count = queries.shape[0]
    scores = jnp.einsum("thk,shk->hts", faded_asking_vector, k_dec, precision=FINEST_ROUNDING)
    scores = scores * jnp.tril(jnp.ones((tok_count, tok_count), jnp.float32))
    inner_part = jnp.einsum("hts,shv->thv", scores, payload_entries, precision=FINEST_ROUNDING)
    external_portion = jnp.einsum(
        "nea,eaw->new", faded_asking_vector, arriving_signal, precision=FINEST_ROUNDING
    )
    return inner_part + external_portion


def span_carry(key_gate, log_forget, payload_entries):
    cumul = jnp.cumsum(log_forget, axis=0)
    final_running_total = cumul[-1]
    scaled_by_factor = key_gate * jnp.exp(final_running_total[None] - cumul)
    return (
        jnp.exp(final_running_total),
        jnp.einsum("xzp,xzo->zpo", scaled_by_factor, payload_entries, precision=FINEST_ROUNDING),
    )


def span_exit(key_gate, log_forget, payload_entries, arriving_signal):
    keep_all, local_sum = span_carry(key_gate, log_forget, payload_entries)
    return keep_all[..., None] * arriving_signal + local_sum


def compose(earlier, later):
    return (earlier[0] * later[0], later[0][..., None] * earlier[1] + later[1])


def normed(mixed, gain):
    mean_square = jnp.mean(mixed * mixed, axis=-1, keepdims=True)
    return mixed * lax.rsqrt(mean_square + NORM_EPS) * gain


def body(block_input, w_query, w_forget_fwd, w_forget_bwd, w_value, floor_rate, gain, cotangent):
    tok_rows, in_width = block_input.shape
    head_count = w_query.shape[1] // KDIM
    val_dim = w_value.shape[1] // head_count
    seq_total = tok_rows * lax.axis_size(SP)
    q_scale = KDIM ** (-0.5)
    norm_scale = seq_total ** (-0.5)

    def project(weight, per_head):
        pre = jnp.dot(block_input, weight, preferred_element_type=jnp.float32).astype(jnp.bfloat16)
        return (
            lax.optimization_barrier(pre)
            .astype(jnp.float32)
            .reshape(tok_rows, head_count, per_head)
        )

    queries = project(w_query, KDIM) * q_scale
    payload_entries = project(w_value, val_dim)
    raw_fwd = project(w_forget_fwd, KDIM)
    raw_bwd = project(w_forget_bwd, KDIM)
    floor_rates = floor_rate.reshape(2, head_count, KDIM)

    def gate_both(gate_fwd, gate_bwd, rate_pair):
        return gate_maps(gate_fwd, rate_pair[0], float(seq_total)) + gate_maps(
            gate_bwd, rate_pair[1], float(seq_total)
        )

    gate_vals, gate_back = jax.vjp(gate_both, raw_fwd, raw_bwd, floor_rates)
    key_fwd, logf_fwd, key_bwd, logf_bwd = gate_vals
    flipped = partial(jnp.flip, axis=0)
    rev_query = flipped(queries)
    rev_key = flipped(key_bwd)
    rev_logf = flipped(logf_bwd)
    rev_value = flipped(payload_entries)
    identity = (
        jnp.ones((head_count, KDIM), jnp.float32),
        jnp.zeros((head_count, KDIM, val_dim), jnp.float32),
    )
    carry_fwd = span_carry(key_fwd, logf_fwd, payload_entries)
    carry_bwd = span_carry(rev_key, rev_logf, rev_value)
    inflow_fwd = entering(carry_fwd, SP, compose, identity, False)[1]
    inflow_bwd = entering(carry_bwd, SP, compose, identity, True)[1]
    mixed_fwd, back_fwd = jax.vjp(
        span_output, queries, key_fwd, logf_fwd, payload_entries, inflow_fwd
    )
    mixed_bwd, back_bwd = jax.vjp(span_output, rev_query, rev_key, rev_logf, rev_value, inflow_bwd)
    mixed = mixed_fwd + flipped(mixed_bwd)
    _, norm_back = jax.vjp(partial(normed, gain=gain), mixed)
    (d_mixed,) = norm_back(cotangent.astype(jnp.float32).reshape(tok_rows, head_count, val_dim))
    dq_fwd, dk_fwd, dlf_fwd, dv_fwd, seed_fwd = back_fwd(d_mixed)
    dq_bwd, dk_bwd, dlf_bwd, dv_bwd, seed_bwd = back_bwd(flipped(d_mixed))
    grad_q = ((dq_fwd + flipped(dq_bwd)) * q_scale).reshape(tok_rows, -1).astype(jnp.bfloat16)
    w_rows = in_width // lax.axis_size(SP)

    def weight_term(first_row, row_count):
        columns = lax.dynamic_slice_in_dim(block_input, first_row, row_count, 1)
        return lax.dot_general(
            columns, grad_q, (((0,), (0,)), ((), ())), preferred_element_type=jnp.float32
        )

    weight_sum = summed_rows(weight_term, w_rows, SP)
    outflow_fwd = entering((carry_fwd[0], seed_fwd), SP, compose, identity, True)[1]
    outflow_bwd = entering((carry_bwd[0], seed_bwd), SP, compose, identity, False)[1]
    _, exit_fwd = jax.vjp(span_exit, key_fwd, logf_fwd, payload_entries, inflow_fwd)
    _, exit_bwd = jax.vjp(span_exit, rev_key, rev_logf, rev_value, inflow_bwd)
    ek_fwd, elf_fwd, ev_fwd, _ = exit_fwd(outflow_fwd)
    ek_bwd, elf_bwd, ev_bwd, _ = exit_bwd(outflow_bwd)
    d_values = dv_fwd + ev_fwd + flipped(dv_bwd + ev_bwd)
    d_raw_fwd, d_raw_bwd, d_rates = gate_back(
        (dk_fwd + ek_fwd, dlf_fwd + elf_fwd, flipped(dk_bwd + ek_bwd), flipped(dlf_bwd + elf_bwd))
    )
    grad_weight = weight_sum * norm_scale
    grad_parts = (
        grad_q,
        d_raw_fwd.reshape(tok_rows, -1).astype(jnp.bfloat16),
        d_raw_bwd.reshape(tok_rows, -1).astype(jnp.bfloat16),
        d_values.reshape(tok_rows, -1).astype(jnp.bfloat16),
    )
    weight_parts = (w_query, w_forget_fwd, w_forget_bwd, w_value)

    def input_term(first_row, row_count):
        summed = jnp.zeros((row_count, in_width), jnp.float32)
        for grad_part, weight in zip(grad_parts, weight_parts):
            rows_part = lax.dynamic_slice_in_dim(grad_part, first_row, row_count, 0)
            summed = summed + lax.dot_general(
                rows_part, weight, (((1,), (1,)), ((), ())), preferred_element_type=jnp.float32
            )
        return summed

    grad_input = summed_rows(input_term, tok_rows // lax.axis_size("tp"), "tp").astype(jnp.bfloat16)
    grad_floor = one_axis_at_a_time(d_rates.reshape(2, -1), SP) * norm_scale
    return (grad_input, grad_weight, grad_floor)


def solution(mesh):
    finer = Mesh(mesh.devices.reshape(4, 4, 2, mesh.shape["tp"]), ("sp_0", "sp_1", "sp_2", "tp"))
    return jax.shard_map(
        body,
        mesh=finer,
        in_specs=(
            P(SP, None),
            P(None, "tp"),
            P(None, "tp"),
            P(None, "tp"),
            P(None, "tp"),
            P(None, "tp"),
            P(),
            P(SP, "tp"),
        ),
        out_specs=(P(SP_TP, None), P(SP, "tp"), P(None, "tp")),
        check_vma=False,
    )
```

profile of v0, /device:TPU:1, one launch (start us, length us, event | category | flops | bytes accessed | tf_op | source)
XLA Modules:
  0.0 357.0 jit_solution(10930753792484951539)
XLA Ops:
  9.1 1.4 convolution_convert_fusion.1
  11.8 1.3 broadcast_multiply_fusion.1
  14.7 2.8 all_gather.103
  18.1 7.9 %all_gather.104 = f32[4,2,128]{2,1,0:T(2,128)S(1)} all-gather(f32[1,2,128]{2,1,0:T(2,128)S(1)} %get-tuple-element.137), channel_id=1, replica_groups=mesh['sp_0'=4,'sp_1'=4,'sp_2'=2,'tp'=4] {'sp_1'}, dimensions={0}, use_global_device_ids=true | all-gather | bytes 5120 | tf_op jit(solution)/shard_map/all_gather | solution.py:29
  26.6 3.8 %all_gather.96 = f32[2,2,128]{2,1,0:T(2,128)S(1)} all-gather(f32[1,2,128]{2,1,0:T(2,128)S(1)} %get-tuple-element.96), channel_id=1, replica_groups=mesh['sp_0'=4,'sp_1'=4,'sp_2'=2,'tp'=4] {'sp_2'}, dimensions={0}, use_global_device_ids=true | all-gather | bytes 3072 | tf_op jit(solution)/shard_map/all_gather | solution.py:29
  30.9 5.4 %all_gather.97 = f32[4,2,128]{2,1,0:T(2,128)S(1)} all-gather(f32[1,2,128]{2,1,0:T(2,128)S(1)} %get-tuple-element.142), channel_id=1, replica_groups=mesh['sp_0'=4,'sp_1'=4,'sp_2'=2,'tp'=4] {'sp_1'}, dimensions={0}, use_global_device_ids=true | all-gather | bytes 5120 | tf_op jit(solution)/shard_map/all_gather | solution.py:29
  39.3 0.9 fusion.144
  41.9 1.1 reverse_multiply_fusion
  43.7 3.6 %all-gather.1 = f32[4,128,128]{2,1,0:T(8,128)S(1)} all-gather(f32[2,128,128]{2,1,0:T(8,128)S(1)} %fusion.114), channel_id=3, replica_groups=mesh['sp_0'=4,'sp_1'=4,'sp_2'=2,'tp'=4] {'sp_2'}, dimensions={0}, use_global_device_ids=true | all-gather | bytes 393216 | tf_op jit(solution)/shard_map/all_gather | solution.py:29
  47.4 10.2 %all_gather.108 = f32[4,2,128,128]{3,2,1,0:T(8,128)S(1)} all-gather(f32[1,2,128,128]{3,2,1,0:T(8,128)S(1)} %bitcast_add_fusion.16), channel_id=1, replica_groups=mesh['sp_0'=4,'sp_1'=4,'sp_2'=2,'tp'=4] {'sp_1'}, dimensions={0}, use_global_device_ids=true | all-gather | bytes 655360 | tf_op jit(solution)/shard_map/all_gather | solution.py:29
  58.5 11.2 %all_gather.109 = f32[4,2,128,128]{3,2,1,0:T(8,128)} all-gather(f32[1,2,128,128]{3,2,1,0:T(8,128)S(1)} %multiply_add_fusion.2), channel_id=1, replica_groups=mesh['sp_0'=4,'sp_1'=4,'sp_2'=2,'tp'=4] {'sp_0'}, dimensions={0}, use_global_device_ids=true | all-gather | bytes 655360 | tf_op jit(solution)/shard_map/all_gather | solution.py:29
  70.3 8.9 %all_gather.105 = f32[4,2,128]{2,1,0:T(2,128)S(1)} all-gather(f32[1,2,128]{2,1,0:T(2,128)S(1)} %copy-done.94), channel_id=1, replica_groups=mesh['sp_0'=4,'sp_1'=4,'sp_2'=2,'tp'=4] {'sp_0'}, dimensions={0}, use_global_device_ids=true | all-gather | bytes 5120 | tf_op jit(solution)/shard_map/all_gather | solution.py:29
  83.6 8.0 %all-gather = f32[4,128,128]{2,1,0:T(8,128)S(1)} all-gather(f32[2,128,128]{2,1,0:T(8,128)S(1)} %fusion.117), channel_id=2, replica_groups=mesh['sp_0'=4,'sp_1'=4,'sp_2'=2,'tp'=4] {'sp_2'}, dimensions={0}, use_global_device_ids=true | all-gather | bytes 393216 | tf_op jit(solution)/shard_map/all_gather | solution.py:29
  92.4 10.8 %all_gather.101 = f32[4,2,128,128]{3,2,1,0:T(8,128)S(1)} all-gather(f32[1,2,128,128]{3,2,1,0:T(8,128)S(1)} %bitcast_add_fusion.22), channel_id=1, replica_groups=mesh['sp_0'=4,'sp_1'=4,'sp_2'=2,'tp'=4] {'sp_1'}, dimensions={0}, use_global_device_ids=true | all-gather | bytes 655360 | tf_op jit(solution)/shard_map/all_gather | solution.py:29
  104.1 10.7 %all_gather.102 = f32[4,2,128,128]{3,2,1,0:T(8,128)} all-gather(f32[1,2,128,128]{3,2,1,0:T(8,128)S(1)} %multiply_add_fusion.3), channel_id=1, replica_groups=mesh['sp_0'=4,'sp_1'=4,'sp_2'=2,'tp'=4] {'sp_0'}, dimensions={0}, use_global_device_ids=true | all-gather | bytes 655360 | tf_op jit(solution)/shard_map/all_gather | solution.py:29
  115.5 5.2 %all_gather.98 = f32[4,2,128]{2,1,0:T(2,128)S(1)} all-gather(f32[1,2,128]{2,1,0:T(2,128)S(1)} %copy-done.93), channel_id=1, replica_groups=mesh['sp_0'=4,'sp_1'=4,'sp_2'=2,'tp'=4] {'sp_0'}, dimensions={0}, use_global_device_ids=true | all-gather | bytes 5120 | tf_op jit(solution)/shard_map/all_gather | solution.py:29
  121.3 1.0 copy.766
  123.8 1.6 fusion.49
  128.1 1.0 multiply_reduce_fusion.7
  130.0 1.1 fusion.82
  131.1 1.1 fusion.79
  132.5 1.0 fusion.182
  133.6 0.9 fusion.120
  135.2 0.9 fusion.94
  137.1 1.0 fusion.180
  138.1 0.9 fusion.77
  139.1 0.9 fusion.89
  140.0 8.8 %all-gather.3 = f32[4,128,128]{2,1,0:T(8,128)S(1)} all-gather(f32[2,128,128]{2,1,0:T(8,128)S(1)} %copy-done.25), channel_id=5, replica_groups=mesh['sp_0'=4,'sp_1'=4,'sp_2'=2,'tp'=4] {'sp_2'}, dimensions={0}, use_global_device_ids=true | all-gather | bytes 393216 | tf_op jit(solution)/shard_map/all_gather | solution.py:29
  149.6 12.0 %all_gather.118 = f32[4,2,128,128]{3,2,1,0:T(8,128)S(1)} all-gather(f32[1,2,128,128]{3,2,1,0:T(8,128)S(1)} %bitcast_add_fusion.4), channel_id=1, replica_groups=mesh['sp_0'=4,'sp_1'=4,'sp_2'=2,'tp'=4] {'sp_1'}, dimensions={0}, use_global_device_ids=true | all-gather | bytes 655360 | tf_op jit(solution)/shard_map/all_gather | solution.py:29
  162.5 11.2 %all_gather.119 = f32[4,2,128,128]{3,2,1,0:T(8,128)S(1)} all-gather(f32[1,2,128,128]{3,2,1,0:T(8,128)S(1)} %multiply_add_fusion), channel_id=1, replica_groups=mesh['sp_0'=4,'sp_1'=4,'sp_2'=2,'tp'=4] {'sp_0'}, dimensions={0}, use_global_device_ids=true | all-gather | bytes 655360 | tf_op jit(solution)/shard_map/all_gather | solution.py:29
  174.3 6.1 %all_gather.115 = f32[4,2,128]{2,1,0:T(2,128)S(1)} all-gather(f32[1,2,128]{2,1,0:T(2,128)S(1)} %copy-done.92), channel_id=1, replica_groups=mesh['sp_0'=4,'sp_1'=4,'sp_2'=2,'tp'=4] {'sp_0'}, dimensions={0}, use_global_device_ids=true | all-gather | bytes 5120 | tf_op jit(solution)/shard_map/all_gather | solution.py:29
  181.1 1.1 multiply_reduce_fusion.4
  183.3 7.8 %all-gather.2 = f32[4,128,128]{2,1,0:T(8,128)S(1)} all-gather(f32[2,128,128]{2,1,0:T(8,128)S(1)} %fusion.91), channel_id=4, replica_groups=mesh['sp_0'=4,'sp_1'=4,'sp_2'=2,'tp'=4] {'sp_2'}, dimensions={0}, use_global_device_ids=true | all-gather | bytes 393216 | tf_op jit(solution)/shard_map/all_gather | solution.py:29
  192.0 11.4 %all_gather.113 = f32[4,2,128,128]{3,2,1,0:T(8,128)S(1)} all-gather(f32[1,2,128,128]{3,2,1,0:T(8,128)S(1)} %bitcast_add_fusion.10), channel_id=1, replica_groups=mesh['sp_0'=4,'sp_1'=4,'sp_2'=2,'tp'=4] {'sp_1'}, dimensions={0}, use_global_device_ids=true | all-gather | bytes 655360 | tf_op jit(solution)/shard_map/all_gather | solution.py:29
  204.3 10.5 %all_gather.114 = f32[4,2,128,128]{3,2,1,0:T(8,128)S(1)} all-gather(f32[1,2,128,128]{3,2,1,0:T(8,128)S(1)} %multiply_add_fusion.1), channel_id=1, replica_groups=mesh['sp_0'=4,'sp_1'=4,'sp_2'=2,'tp'=4] {'sp_0'}, dimensions={0}, use_global_device_ids=true | all-gather | bytes 655360 | tf_op jit(solution)/shard_map/all_gather | solution.py:29
  215.5 5.4 %all_gather.110 = f32[4,2,128]{2,1,0:T(2,128)S(1)} all-gather(f32[1,2,128]{2,1,0:T(2,128)S(1)} %copy-done.91), channel_id=1, replica_groups=mesh['sp_0'=4,'sp_1'=4,'sp_2'=2,'tp'=4] {'sp_0'}, dimensions={0}, use_global_device_ids=true | all-gather | bytes 5120 | tf_op jit(solution)/shard_map/all_gather | solution.py:29
  226.8 1.1 fusion.104
  228.0 1.4 fusion.175
  230.1 1.0 multiply_reduce_fusion
  231.5 1.1 fusion.108
  233.3 2.4 fusion.167
  239.3 1.1 convolution_add_fusion
  240.8 1.4 copy.790
  244.3 7.5 %psum.21 = f32[2,256]{1,0:T(2,128)S(1)} all-reduce(f32[2,256]{1,0:T(2,128)S(1)} %bitcast.638), channel_id=1, replica_groups=mesh['sp_0'=4,'sp_1'=4,'sp_2'=2,'tp'=4] {'sp_0'}, use_global_device_ids=true, to_apply=%region_20.22 | all-reduce | flops 512 | bytes 4096 | tf_op jit(solution)/shard_map/psum | solution.py:46
  251.7 6.9 %psum.22 = f32[2,256]{1,0:T(2,128)S(1)} all-reduce(f32[2,256]{1,0:T(2,128)S(1)} %psum.21), channel_id=1, replica_groups=mesh['sp_0'=4,'sp_1'=4,'sp_2'=2,'tp'=4] {'sp_1'}, use_global_device_ids=true, to_apply=%region_21.23 | all-reduce | flops 512 | bytes 4096 | tf_op jit(solution)/shard_map/psum | solution.py:46
  258.7 14.6 %psum.23 = f32[2,256]{1,0:T(2,128)S(1)} all-reduce(f32[2,256]{1,0:T(2,128)S(1)} %psum.22), channel_id=1, replica_groups=mesh['sp_0'=4,'sp_1'=4,'sp_2'=2,'tp'=4] {'sp_2'}, use_global_device_ids=true, to_apply=%region_22.24 | all-reduce | flops 512 | bytes 4096 | tf_op jit(solution)/shard_map/psum | solution.py:46
  273.9 1.5 convert_element_type.56
  275.4 73.2 %reduce-scatter.7.cloned.1.call-done = f32[32,256]{1,0:T(8,128)} async-done(((f32[1024,256]{1,0:T(8,128)}), f32[32,256]{1,0:T(8,128)}) %reduce-scatter.7.cloned.1.call-update) | async-done | bytes 32784
  (289 shorter events, 49.4 us)
Async XLA Ops:
  7.2 33.0 %copy-start = (bf16[1024,256]{1,0:T(8,128)(2,1)S(1)}, bf16[1024,256]{1,0:T(8,128)(2,1)}, u32[]{:S(2)}) copy-start(bf16[1024,256]{1,0:T(8,128)(2,1)} %param.10) | copy-start | bytes 1572868
  7.2 266.7 %reduce-scatter.5.cloned.1.call-start = ((), (), s32[]{:S(2)}) async-start(), calls=%async_computation.2 | async-start | bytes 655360 | tf_op jit(solution)/shard_map/reduce_scatter | solution.py:41
  8.6 3.0 copy-start.41
  8.6 5.5 %copy-start.39 = (f32[1,256]{1,0:T(1,128)}, f32[1,256]{1,0:T(1,128)S(1)}, u32[]{:S(2)}) copy-start(f32[1,256]{1,0:T(1,128)S(1)} %get-tuple-element.58) | copy-start | bytes 3076
  9.1 4.9 %copy-start.62 = (f32[2,128]{1,0:T(2,128)}, f32[2,128]{1,0:T(2,128)S(1)}, u32[]{:S(2)}) copy-start(f32[2,128]{1,0:T(2,128)S(1)} %get-tuple-element.149) | copy-start | bytes 3076
  9.1 2.1 copy-start.1
  9.1 2.1 copy-start.3
  11.5 1.6 copy-start.7
  14.0 27.6 %copy-start.47 = (f32[2,128]{1,0:T(2,128)}, f32[2,128]{1,0:T(2,128)S(1)}, u32[]{:S(2)}) copy-start(f32[2,128]{1,0:T(2,128)S(1)} %get-tuple-element.99) | copy-start | bytes 3076
  14.7 26.9 %copy-start.43 = (f32[2,128]{1,0:T(2,128)}, f32[2,128]{1,0:T(2,128)S(1)}, u32[]{:S(2)}) copy-start(f32[2,128]{1,0:T(2,128)S(1)} %get-tuple-element.97) | copy-start | bytes 3076
  18.1 29.1 %copy-start.56 = (f32[2,128]{1,0:T(2,128)}, f32[2,128]{1,0:T(2,128)S(1)}, u32[]{:S(2)}) copy-start(f32[2,128]{1,0:T(2,128)S(1)} %get-tuple-element.136) | copy-start | bytes 3076
  38.8 8.5 %copy-start.72 = (f32[2,128]{1,0:T(2,128)}, f32[2,128]{1,0:T(2,128)S(1)}, u32[]{:S(2)}) copy-start(f32[2,128]{1,0:T(2,128)S(1)} %get-tuple-element.134) | copy-start | bytes 3076
  40.2 1.0 copy-start.4
  43.0 36.9 %copy-start.9 = (f32[128,2,128]{2,1,0:T(2,128)}, f32[128,2,128]{2,1,0:T(2,128)S(1)}, u32[]{:S(2)}) copy-start(f32[128,2,128]{2,1,0:T(2,128)S(1)} %get-tuple-element.91) | copy-start | bytes 393220
  43.0 40.3 %copy-start.20 = (f32[128,2,128]{2,1,0:T(2,128)}, f32[128,2,128]{2,1,0:T(2,128)S(1)}, u32[]{:S(2)}) copy-start(f32[128,2,128]{2,1,0:T(2,128)S(1)} %get-tuple-element.94) | copy-start | bytes 393220
  47.4 10.3 %copy-start.58 = (f32[2,128]{1,0:T(2,128)S(1)}, f32[2,128]{1,0:T(2,128)}, u32[]{:S(2)}) copy-start(f32[2,128]{1,0:T(2,128)} %get-tuple-element.107) | copy-start | bytes 3076
  47.4 10.2 %copy-start.70 = (f32[2,128]{1,0:T(2,128)S(1)}, f32[2,128]{1,0:T(2,128)}, u32[]{:S(2)}) copy-start(f32[2,128]{1,0:T(2,128)} %get-tuple-element.112) | copy-start | bytes 3076
  79.9 1.1 copy-start.6
  83.6 8.0 %copy-start.69 = (f32[2,128]{1,0:T(2,128)S(1)}, f32[2,128]{1,0:T(2,128)}, u32[]{:S(2)}) copy-start(f32[2,128]{1,0:T(2,128)} %get-tuple-element.139) | copy-start | bytes 3076
  92.4 10.9 %copy-start.68 = (f32[2,128]{1,0:T(2,128)S(1)}, f32[2,128]{1,0:T(2,128)}, u32[]{:S(2)}) copy-start(f32[2,128]{1,0:T(2,128)} %get-tuple-element.124) | copy-start | bytes 3076
  121.3 1.0 copy-start.31
  132.5 1.1 copy-start.10
  137.1 1.1 copy-start.12
  139.1 0.9 copy-start.25
  140.0 8.8 %copy-start.67 = (f32[2,128]{1,0:T(2,128)S(1)}, f32[2,128]{1,0:T(2,128)}, u32[]{:S(2)}) copy-start(f32[2,128]{1,0:T(2,128)} %get-tuple-element.133) | copy-start | bytes 3076
  149.6 12.0 %copy-start.52 = (f32[2,128]{1,0:T(2,128)S(1)}, f32[2,128]{1,0:T(2,128)}, u32[]{:S(2)}) copy-start(f32[2,128]{1,0:T(2,128)} %get-tuple-element.110) | copy-start | bytes 3076
  149.6 12.0 %copy-start.66 = (f32[2,128]{1,0:T(2,128)S(1)}, f32[2,128]{1,0:T(2,128)}, u32[]{:S(2)}) copy-start(f32[2,128]{1,0:T(2,128)} %get-tuple-element.111) | copy-start | bytes 3076
  162.4 18.0 %copy-start.90 = (f32[2,128]{1,0:T(2,128)S(1)}, f32[2,128]{1,0:T(2,128)}, u32[]{:S(2)}) copy-start(f32[2,128]{1,0:T(2,128)} %get-tuple-element.64) | copy-start | bytes 3076
  183.3 7.9 %copy-start.65 = (f32[2,128]{1,0:T(2,128)S(1)}, f32[2,128]{1,0:T(2,128)}, u32[]{:S(2)}) copy-start(f32[2,128]{1,0:T(2,128)} %get-tuple-element.138) | copy-start | bytes 3076
  192.0 11.4 %copy-start.64 = (f32[2,128]{1,0:T(2,128)S(1)}, f32[2,128]{1,0:T(2,128)}, u32[]{:S(2)}) copy-start(f32[2,128]{1,0:T(2,128)} %get-tuple-element.123) | copy-start | bytes 3076
  204.3 16.6 %copy-start.88 = (f32[2,128]{1,0:T(2,128)S(1)}, f32[2,128]{1,0:T(2,128)}, u32[]{:S(2)}) copy-start(f32[2,128]{1,0:T(2,128)} %get-tuple-element.70) | copy-start | bytes 3076
  223.3 1.0 copy-start.30
  224.6 0.9 copy-start.22
  224.6 1.0 copy-start.23
  226.8 1.2 copy-start.33
  226.8 1.2 copy-start.34
  227.9 1.5 copy-start.8
  228.0 1.5 copy-start.19
  228.0 1.5 copy-start.46
  228.0 1.5 copy-start.74
  231.1 1.5 copy-start.63
  231.1 1.5 copy-start.75
  231.5 1.2 copy-start.14
  233.3 2.4 copy-start.21
  233.3 2.4 copy-start.29
  235.7 1.0 copy-start.2
  238.3 1.0 copy-start.5
  240.5 108.1 %reduce-scatter.7.cloned.1.call-start = ((), (), s32[]{:S(2)}) async-start(), calls=%async_computation.3 | async-start | bytes 1081344
  (53 other events, 37.7 us)
Sparse Core Ops, SparseCore 0:
  240.6 26.2 reduce-scatter.4
  270.4 78.1 reduce-scatter.6
where the time goes:
time: 359 us; the launch traced here: 357 us
  blocking collectives  191 us (53%)
  waiting for transfers between devices  73.2 us (20%)
  local copies, waits for them, and re-layouts  31.1 us (9%)
  other arithmetic  28 us (8%)
  matrix products  18.7 us (5%)
  between operations  15.1 us (4%)
    all_gather x20, blocking collectives, entering(): pieces = jax.tree.map(lambda part: lax.all_gather(part, axis), subtotal)  162 us
    unnamed x3, waiting for transfers between devices  73.2 us
    psum x3, blocking collectives, one_axis_at_a_time(): array = lax.psum(array, axis)  29 us
    unnamed x202, local copies, waits for them, and re-layouts  26.4 us
  transfers between devices with their start and end apart: 2, of which 1 were waited for; matrix products, arithmetic and copies ran while one was open for 1% of the time, Pallas kernels for 0%

commit v1 on v0

v1 whole, which is shorter than its diff:
```python
import jax
import jax.numpy as jnp
from jax import lax
from jax.experimental import pallas as pl
from jax.experimental.pallas import tpu as pltpu
from jax.sharding import Mesh
from jax.sharding import PartitionSpec as P

SP = ("sp_0", "sp_1", "sp_2")
SP_TP = ("sp_0", "sp_1", "sp_2", "tp")
N = 32
T = 128
K = 128
HEADS = 2
W = HEADS * K
D = 1024
TOKENS = 4096.0
Q_SCALE = K ** (-0.5)
OUT_SCALE = TOKENS ** (-0.5)
NORM_EPS = 1e-06
F32 = jnp.float32
BF16 = jnp.bfloat16
NN = ((1,), (0,))
NT = ((1,), (1,))
VMEM = pl.BlockSpec(memory_space=pltpu.VMEM)
SMEM = pl.BlockSpec(memory_space=pltpu.SMEM)


def dot(a, b, dims):
    return lax.dot_general(a, b, (dims, ((), ())), preferred_element_type=F32)


def split(a):
    high = a.astype(BF16)
    return high, (a - high.astype(F32)).astype(BF16)


def dot3(a, b, dims):
    (ah, al), (bh, bl) = split(a), split(b)
    return dot(ah, bh, dims) + (dot(ah, bl, dims) + dot(al, bh, dims))


def dot2(a, b, dims):
    bh, bl = split(b)
    return dot(a, bh, dims) + dot(a, bl, dims)


def dot2r(a, b, dims):
    ah, al = split(a)
    return dot(ah, b, dims) + dot(al, b, dims)


def lower_triangle():
    row = lax.broadcasted_iota(jnp.int32, (T, T), 0)
    col = lax.broadcasted_iota(jnp.int32, (T, T), 1)
    return row >= col, row <= col


def opening_of(rate):
    r = rate * (1.0 / TOKENS)
    return r * (1.0 - r * (1 / 2) * (1.0 - r * (1 / 3) * (1.0 - r * (1 / 4))))


def gates(raw, opening):
    x = raw.astype(F32)
    closed = 1.0 / (1.0 + jnp.exp(x))
    return closed, opening * closed


def log_forget_of(key):
    return -key * (1.0 + key * (1 / 2 + key * (1 / 3 + key * (1 / 4 + key * (1 / 5)))))


def project_kernel(x_ref, wq_ref, wf_ref, wb_ref, wv_ref, rate_ref, q_ref, f_ref, b_ref, v_ref, cf_ref, cb_ref, msg_ref):
    x = x_ref[...]
    low, up = lower_triangle()
    low, up = low.astype(BF16), up.astype(BF16)
    v = dot(x, wv_ref[...], NN).astype(BF16)
    v_ref[...] = v
    opening = opening_of(rate_ref[...])
    decayed = []
    for d, (w_ref, raw_ref, cum_ref, tri) in enumerate(((wf_ref, f_ref, cf_ref, low), (wb_ref, b_ref, cb_ref, up))):
        raw = dot(x, w_ref[...], NN).astype(BF16)
        raw_ref[...] = raw
        _, key = gates(raw, opening[d : d + 1])
        cum = dot2(tri, log_forget_of(key), NN)
        cum_ref[...] = cum
        last = cum[T - 1 : T] if d == 0 else cum[0:1]
        decayed.append((jnp.exp(last), key * jnp.exp(last - cum)))
    for h in range(HEADS):
        cols = slice(h * K, (h + 1) * K)
        v_t = v[:, cols].astype(F32).T.astype(BF16)
        group = slice(h * 16, (h + 1) * 16)
        msg_ref[group, 16:24, :] = jnp.zeros((16, 8, K), F32)
        for d, (all_keep, left) in enumerate(decayed):
            state = dot2(v_t, left[:, cols], NN)
            msg_ref[group, 8 * d : 8 * d + 8, :] = state.reshape(16, 8, K)
            msg_ref[group, 16 + d : 17 + d, :] = jnp.broadcast_to(all_keep[:, cols].reshape(1, 1, K), (16, 1, K))
    q_ref[...] = dot(x, wq_ref[...], NN).astype(BF16)


def scan_kernel(got_ref, out_ref):
    run = jnp.zeros((8, K), F32)
    for j in range(N):
        out_ref[j, 0:8, :] = run
        run = got_ref[j, 16:17, :] * run + got_ref[j, 0:8, :]
    run = jnp.zeros((8, K), F32)
    for j in reversed(range(N)):
        out_ref[j, 8:16, :] = run
        run = got_ref[j, 17:18, :] * run + got_ref[j, 8:16, :]


def mix_kernel(
    core_ref, x_ref, q_ref, f_ref, b_ref, v_ref, cf_ref, cb_ref, rate_ref, gain_ref, cot_ref, in_ref,
    msg_ref, own_ref, other_ref, gq_ref, dv_ref, dbf_ref, dbb_ref, af_ref, ab_ref,
):
    low, up = lower_triangle()
    opening = opening_of(rate_ref[...])
    gain = gain_ref[...]
    grad_q = []
    for h in range(HEADS):
        cols = slice(h * K, (h + 1) * K)
        group = slice(h * 16, (h + 1) * 16)
        q = q_ref[:, cols].astype(F32) * Q_SCALE
        v = v_ref[:, cols]
        v_t = v.astype(F32).T.astype(BF16)
        parts = []
        for d, (raw_ref, cum_ref, tri) in enumerate(((f_ref, cf_ref, low), (b_ref, cb_ref, up))):
            closed, key = gates(raw_ref[:, cols], opening[d : d + 1, cols])
            cum = cum_ref[:, cols]
            grow = jnp.exp(cum)
            fade = jnp.exp(-cum)
            last = cum[T - 1 : T] if d == 0 else cum[0:1]
            state = in_ref[group, 8 * d : 8 * d + 8, :].reshape(K, K)
            parts.append((closed, key, grow, fade, last, q * grow, key * fade, state, tri))
        scores = jnp.zeros((T, T), F32)
        mixed = jnp.zeros((T, K), F32)
        for closed, key, grow, fade, last, a, b, state, tri in parts:
            scores = scores + jnp.where(tri, dot3(a, b, NT), 0.0)
            mixed = mixed + dot3(a, state, NT)
        mixed = mixed + dot2r(scores, v, NN)
        inv = lax.rsqrt(jnp.mean(mixed * mixed, axis=-1, keepdims=True) + NORM_EPS)
        scaled = cot_ref[:, cols].astype(F32) * gain
        d_mixed = inv * scaled - mixed * (inv * inv * inv * jnp.mean(scaled * mixed, axis=-1, keepdims=True))
        d_mixed_t = d_mixed.T
        d_scores = dot2r(d_mixed, v, NT)
        dv_ref[:, cols] = dot3(scores.T, d_mixed, NN)
        dq = jnp.zeros((T, K), F32)
        msg_ref[group, 32:40, :] = jnp.zeros((16, 8, K), F32)
        for d, (closed, key, grow, fade, last, a, b, state, tri) in enumerate(parts):
            local = jnp.where(tri, d_scores, 0.0)
            da = dot3(local, b, NN) + dot3(d_mixed, state, NN)
            db = dot3(local.T, a, NN)
            dq = dq + da * grow
            ada = a * da
            (dbf_ref, dbb_ref)[d][:, cols] = db
            (af_ref, ab_ref)[d][:, cols] = ada
            seed = dot3(d_mixed_t, a, NN)
            msg_ref[group, 8 * d : 8 * d + 8, :] = seed.reshape(16, 8, K)
            share = closed / (1.0 - key)
            before = dot2(tri.astype(BF16), share, NN)
            total = before[T - 1 : T] if d == 0 else before[0:1]
            keep = jnp.exp(last)
            z = keep * fade * (closed - (total - before) * key)
            reach = dot2(v_t, z, NN) - (keep * total) * state
            msg_ref[group, 16 + 8 * d : 24 + 8 * d, :] = reach.reshape(16, 8, K)
            floor = jnp.sum(closed * (db * fade) - before * (ada - b * db), axis=0, keepdims=True)
            msg_ref[h * 16, 32 + d : 33 + d, :] = floor
        grad_q.append((dq * Q_SCALE).astype(BF16))
    gq = jnp.concatenate(grad_q, axis=1)
    gq_ref[...] = gq
    term = dot(x_ref[...].astype(F32).T.astype(BF16), gq, NN).reshape(N, 2, 16, W)
    first = core_ref[0] == 0
    own = jnp.where(first, term[:, 0], term[:, 1])
    other = jnp.where(first, term[:, 1], term[:, 0])
    for part, ref in ((own, own_ref), (other, other_ref)):
        for h in range(HEADS):
            ref[:, 16 * h : 16 * h + 16, :] = part[:, :, h * K : (h + 1) * K]


def scan_back_kernel(keep_ref, got_ref, own_ref, other_ref, out_ref):
    run = jnp.zeros((8, K), F32)
    reach = jnp.zeros((8, K), F32)
    floor = jnp.zeros((1, K), F32)
    for j in reversed(range(N)):
        out_ref[j, 0:8, :] = run
        reach = reach + run * got_ref[j, 16:24, :]
        floor = floor + got_ref[j, 32:33, :]
        run = keep_ref[j, 16:17, :] * run + got_ref[j, 0:8, :]
    floor_fwd = floor + jnp.sum(reach, axis=0, keepdims=True)
    run = jnp.zeros((8, K), F32)
    reach = jnp.zeros((8, K), F32)
    floor = jnp.zeros((1, K), F32)
    for j in range(N):
        out_ref[j, 8:16, :] = run
        reach = reach + run * got_ref[j, 24:32, :]
        floor = floor + got_ref[j, 33:34, :]
        run = keep_ref[j, 17:18, :] * run + got_ref[j, 8:16, :]
    floor_bwd = floor + jnp.sum(reach, axis=0, keepdims=True)
    out_ref[:, 16:48, :] = own_ref[...] + other_ref[...]
    tail = jnp.concatenate([floor_fwd, floor_bwd, jnp.zeros((6, K), F32)], axis=0)
    out_ref[:, 48:56, :] = jnp.broadcast_to(tail[None], (N, 8, K))


def finish_kernel(
    f_ref, b_ref, v_ref, cf_ref, cb_ref, rate_ref, in_ref, got_ref,
    gq_ref, dv_ref, dbf_ref, dbb_ref, af_ref, ab_ref, wq_ref, wf_ref, wb_ref, wv_ref,
    term_ref, weight_ref, floor_ref,
):
    low, up = lower_triangle()
    rate = rate_ref[...]
    opening = opening_of(rate)
    g_raw = ([], [])
    g_value = []
    floor_rows = ([], [])
    for h in range(HEADS):
        cols = slice(h * K, (h + 1) * K)
        group = slice(h * 16, (h + 1) * 16)
        v = v_ref[:, cols]
        dv = dv_ref[:, cols]
        for d, (raw_ref, cum_ref, db_ref, ada_ref, rev) in enumerate(
            ((f_ref, cf_ref, dbf_ref, af_ref, up), (b_ref, cb_ref, dbb_ref, ab_ref, low))
        ):
            closed, key = gates(raw_ref[:, cols], opening[d : d + 1, cols])
            opened = 1.0 / (1.0 + jnp.exp(-raw_ref[:, cols].astype(F32)))
            cum = cum_ref[:, cols]
            fade = jnp.exp(-cum)
            last = cum[T - 1 : T] if d == 0 else cum[0:1]
            keep = jnp.exp(last)
            state = in_ref[group, 8 * d : 8 * d + 8, :].reshape(K, K)
            flow = got_ref[group, 8 * d : 8 * d + 8, :].reshape(K, K)
            b = key * fade
            left = b * keep
            d_left = dot2(v, flow, NN)
            dv = dv + dot3(left, flow, NT)
            db = db_ref[:, cols] + keep * d_left
            dc = ada_ref[:, cols] - b * db
            total = jnp.sum(left * d_left, axis=0, keepdims=True) + keep * jnp.sum(state * flow, axis=0, keepdims=True)
            d_log = dot2(rev.astype(BF16), dc, NN) + total
            whole = db * fade - d_log / (1.0 - key)
            g_raw[d].append((-key * opened * whole).astype(BF16))
            floor_rows[d].append(jnp.sum(got_ref[group, 48 + d : 49 + d, :], axis=0))
        g_value.append(dv.astype(BF16))
    out = dot(gq_ref[...], wq_ref[...], NT)
    out = out + dot(jnp.concatenate(g_raw[0], axis=1), wf_ref[...], NT)
    out = out + dot(jnp.concatenate(g_raw[1], axis=1), wb_ref[...], NT)
    out = out + dot(jnp.concatenate(g_value, axis=1), wv_ref[...], NT)
    term_ref[...] = out
    for c in range(2):
        acc = got_ref[c, 16:48, :]
        for j in range(1, N // 2):
            acc = acc + got_ref[2 * j + c, 16:48, :]
        for h in range(HEADS):
            weight_ref[16 * c : 16 * c + 16, h * K : (h + 1) * K] = acc[16 * h : 16 * h + 16] * OUT_SCALE
    shift = jnp.exp(rate * (-1.0 / TOKENS)) * (OUT_SCALE / TOKENS)
    for d in range(2):
        floor_ref[d : d + 1, :] = jnp.concatenate(floor_rows[d], axis=1) * shift[d : d + 1]


def shape(*dims, dtype=F32):
    return jax.ShapeDtypeStruct(dims, dtype)


def call(kernel, out_shape, specs, name):
    many = isinstance(out_shape, (tuple, list))
    return pl.pallas_call(
        kernel,
        out_shape=out_shape,
        in_specs=specs,
        out_specs=[VMEM] * len(out_shape) if many else VMEM,
        name=name,
    )


def exchange(array, axes):
    return lax.all_to_all(array, axes, 0, 0, tiled=True)


def body(x, w_query, w_forget_fwd, w_forget_bwd, w_value, floor_rate, gain, cotangent):
    tok = shape(T, W)
    tok16 = shape(T, W, dtype=BF16)
    q, f, b, v, cf, cb, sums = call(
        project_kernel, (tok16, tok16, tok16, tok16, tok, tok, shape(N, 24, K)), [VMEM] * 6, "project"
    )(x, w_query, w_forget_fwd, w_forget_bwd, w_value, floor_rate)
    sums = exchange(sums, SP)
    inflow = exchange(call(scan_kernel, shape(N, 16, K), [VMEM], "scan")(sums), SP)
    core = lax.axis_index("sp_2").reshape(1).astype(jnp.int32)
    seeds, own, other, gq, dv, dbf, dbb, af, ab = call(
        mix_kernel,
        (shape(N, 40, K), shape(N, 32, K), shape(N, 32, K), tok16, tok, tok, tok, tok, tok),
        [SMEM] + [VMEM] * 11,
        "mix",
    )(core, x, q, f, b, v, cf, cb, floor_rate, gain.reshape(1, K), cotangent, inflow)
    other = lax.ppermute(other, "sp_2", [(0, 1), (1, 0)])
    seeds = exchange(seeds, SP)
    outflow = exchange(
        call(scan_back_kernel, shape(N, 56, K), [VMEM] * 4, "scan_back")(sums, seeds, own, other), SP
    )
    term, grad_weight, grad_floor = call(
        finish_kernel, (shape(T, D), shape(N, W), shape(2, W)), [VMEM] * 18, "finish"
    )(
        f, b, v, cf, cb, floor_rate, inflow, outflow, gq, dv, dbf, dbb, af, ab,
        w_query, w_forget_fwd, w_forget_bwd, w_value,
    )
    pieces = exchange(term, "tp").reshape(4, T // 4, D)
    grad_input = (pieces[0] + pieces[1] + pieces[2] + pieces[3]).astype(BF16)
    return grad_input, grad_weight, grad_floor


def solution(mesh):
    finer = Mesh(mesh.devices.reshape(4, 4, 2, mesh.shape["tp"]), ("sp_0", "sp_1", "sp_2", "tp"))
    return jax.shard_map(
        body,
        mesh=finer,
        in_specs=(
            P(SP, None),
            P(None, "tp"),
            P(None, "tp"),
            P(None, "tp"),
            P(None, "tp"),
            P(None, "tp"),
            P(),
            P(SP, "tp"),
        ),
        out_specs=(P(SP_TP, None), P(SP, "tp"), P(None, "tp")),
        check_vma=False,
    )
```

time: 359 us -> 104 us (0.29)
  blocking collectives: 191 us -> 53.4 us
  waiting for transfers between devices: 73.2 us -> 21.8 us
  local copies, waits for them, and re-layouts: 31.1 us -> 1.53 us
  other arithmetic: 28 us -> 0.66 us
  matrix products: 18.7 us -> 0 us
  Pallas kernels: 0 us -> 17.4 us
  between operations: 15.1 us -> 0.68 us
  starting transfers between devices: 0.08 us -> 8.07 us
    all_gather x20 -> x0, blocking collectives: 162 us -> none  [entering(): pieces = jax.tree.map(lambda part: lax.all_gather(part, axis), subtotal)]
    unnamed x3 -> x0, waiting for transfers between devices: 73.2 us -> none
    all_to_all x0 -> x3, blocking collectives: none -> 53.4 us  [exchange(): return lax.all_to_all(array, axes, 0, 0, tiled=True)]
    psum x3 -> x0, blocking collectives: 29 us -> none  [one_axis_at_a_time(): array = lax.psum(array, axis)]
    unnamed x202 -> x8, local copies, waits for them, and re-layouts: 26.4 us -> 1.53 us
    all_to_all x0 -> x2, waiting for transfers between devices: none -> 20.2 us  [exchange(): return lax.all_to_all(array, axes, 0, 0, tiled=True)]
    dot_general x33 -> x0, matrix products: 18.7 us -> none  [the longest x6 4.19 us: span_output(): jnp.einsum('nea,eaw->new', faded_asking_vector, arriving_signal, precisio...]
    pallas_call x0 -> x5, Pallas kernels: none -> 17.4 us  [the longest x1 5.09 us: body(): call(mix_kernel, (shape(N, 40, K), shape(N, 32, K), shape(N, 32, K), tok1...]
  transfers between devices with their start and end apart: 2 -> 3, of which waited for: 1 -> 3; matrix products, arithmetic and copies ran while one was open for 1% -> 0% of each run, Pallas kernels for 0% -> 0%
where the time goes in v1:
time: 104 us
  blocking collectives  53.4 us (51%)
  waiting for transfers between devices  21.8 us (21%)
  Pallas kernels  17.4 us (17%)
  starting transfers between devices  8.07 us (8%)
  local copies, waits for them, and re-layouts  1.53 us (1%)
    all_to_all x3, blocking collectives, exchange(): return lax.all_to_all(array, axes, 0, 0, tiled=True)  53.4 us
    all_to_all x2, waiting for transfers between devices, exchange(): return lax.all_to_all(array, axes, 0, 0, tiled=True)  20.2 us
    all_to_all x2, starting transfers between devices, exchange(): return lax.all_to_all(array, axes, 0, 0, tiled=True)  7.7 us
    pallas_call x1, Pallas kernels, body(): call(mix_kernel, (shape(N, 40, K), shape(N, 32, K), shape(N, 32, K), tok1...  5.09 us
    pallas_call x1, Pallas kernels, body(): call(finish_kernel, (shape(T, D), shape(N, W), shape(2, W)), [VMEM] * 18,...  4.65 us
    pallas_call x1, Pallas kernels, body(): call(project_kernel, (tok16, tok16, tok16, tok16, tok, tok, shape(N, 24,...  3.34 us
    pallas_call x1, Pallas kernels, body(): call(scan_back_kernel, shape(N, 56, K), [VMEM] * 4, 'scan_back')  2.57 us
  transfers between devices with their start and end apart: 3, of which 3 were waited for; matrix products, arithmetic and copies ran while one was open for 0% of the time, Pallas kernels for 0%

profile of v1, /device:TPU:1, one launch (start us, length us, event | category | flops | bytes accessed | tf_op | source)
XLA Modules:
  0.0 103.6 jit_solution(17809730299763308878)
XLA Ops:
  0.6 3.3 %project.1 = (bf16[128,256]{1,0:T(8,128)(2,1)}, bf16[128,256]{1,0:T(8,128)(2,1)}, bf16[128,256]{1,0:T(8,128)(2,1)}, bf16[128,256]{1,0:T(8,128)(2,1)}, f32[128,25...) custom-call(bf16[128,1024]{1,0:T(8,128)(2,1)} %x_ref.3, bf16[1024,256]{1,0:T(8,128)(2,1)} %wq_ref.3, ...), custom_call_target="tpu_custom_call" | custom-call | tf_op jit(solution)/shard_map/project/pallas_call | solution.py:282
  4.0 18.8 %all_to_all.29.got_ref.keep_ref = f32[32,24,128]{2,1,0:T(8,128)} all-to-all(f32[32,24,128]{2,1,0:T(8,128)} %get-tuple-element.27), channel_id=1, replica_groups=mesh['sp_0'=4,'sp_1'=4,'sp_2'=2,'tp'=4] {'sp_0','sp_1','sp_2'}, dimensions={0} | all-to-all | bytes 786432 | tf_op jit(solution)/shard_map/all_to_all | solution.py:276
  22.8 1.8 %scan.1 = f32[32,16,128]{2,1,0:T(8,128)} custom-call(f32[32,24,128]{2,1,0:T(8,128)} %all_to_all.29.got_ref.keep_ref), custom_call_target="tpu_custom_call" | custom-call | tf_op jit(solution)/shard_map/scan/pallas_call | solution.py:286
  24.6 3.8 %all-to-all-start.1 = ((f32[32,16,128]{2,1,0:T(8,128)}), f32[32,16,128]{2,1,0:T(8,128)S(1)}, u32[]{:S(2)}, u32[]{:S(2)}) async-start(f32[32,16,128]{2,1,0:T(8,128)} %scan.1), calls=%async_computation.1 | async-start | bytes 524288 | tf_op jit(solution)/shard_map/all_to_all | solution.py:276
  28.4 9.0 %all-to-all-done.1.in_ref = f32[32,16,128]{2,1,0:T(8,128)S(1)} async-done(((f32[32,16,128]{2,1,0:T(8,128)}), f32[32,16,128]{2,1,0:T(8,128)S(1)}, u32[]{:S(2)}, u32[]{:S(2)}) %all-to-all-start.1) | async-done | bytes 262176 | tf_op jit(solution)/shard_map/all_to_all | solution.py:276
  37.4 0.0 copy-start.1
  37.4 0.7 copy-done.1
  38.1 5.1 %mix.1 = (f32[32,40,128]{2,1,0:T(8,128)}, f32[32,32,128]{2,1,0:T(8,128)}, f32[32,32,128]{2,1,0:T(8,128)}, bf16[128,256]{1,0:T(8,128)(2,1)}, f32[128,256]{1,0:T(8...) custom-call(s32[1]{0:T(128)} %bitcast.core_ref, ...), custom_call_target="tpu_custom_call" | custom-call | tf_op jit(solution)/shard_map/mix/pallas_call | solution.py:288
  43.2 0.0 copy-start.3
  43.2 3.9 %all-to-all-start.2 = ((f32[32,40,128]{2,1,0:T(8,128)}), f32[32,40,128]{2,1,0:T(8,128)S(1)}, u32[]{:S(2)}, u32[]{:S(2)}) async-start(f32[32,40,128]{2,1,0:T(8,128)} %get-tuple-element.29), calls=%async_computation.2 | async-start | bytes 1310720 | tf_op jit(solution)/shard_map/all_to_all | solution.py:276
  47.1 0.0 copy-done.3
  47.1 0.4 collective-permute-start
  47.5 1.6 %collective-permute-done.other_ref = f32[32,32,128]{2,1,0:T(8,128)S(1)} collective-permute-done((f32[32,32,128]{2,1,0:T(8,128)S(1)}, f32[32,32,128]{2,1,0:T(8,128)S(1)}, u32[]{:S(2)}, u32[]{:S(2)}) %collective-permute-start) | collective-permute-done | bytes 524320 | tf_op jit(solution)/shard_map/ppermute | solution.py:294
  49.1 0.0 copy-start.2
  49.1 11.2 %all-to-all-done.2.got_ref = f32[32,40,128]{2,1,0:T(8,128)S(1)} async-done(((f32[32,40,128]{2,1,0:T(8,128)}), f32[32,40,128]{2,1,0:T(8,128)S(1)}, u32[]{:S(2)}, u32[]{:S(2)}) %all-to-all-start.2) | async-done | bytes 655392 | tf_op jit(solution)/shard_map/all_to_all | solution.py:276
  60.3 0.0 copy-start
  60.3 0.0 copy-done.2
  60.3 0.8 copy-done
  61.1 2.6 %scan_back.1 = f32[32,56,128]{2,1,0:T(8,128)} custom-call(f32[32,24,128]{2,1,0:T(8,128)} %all_to_all.29.got_ref.keep_ref, f32[32,40,128]{2,1,0:T(8,128)} %copy-done, f32[32,32,128]{2,1,0:T(8,128)} %get-tuple-element.30.own_ref, f32[32,32,128]{2,1,0:T(8,128)} %copy-done.2), custom_call_target="tpu_custom_call" | custom-call | tf_op jit(solution)/shard_map/scan_back/pallas_call | solution.py:297
  63.7 20.3 %all_to_all.30.got_ref = f32[32,56,128]{2,1,0:T(8,128)} all-to-all(f32[32,56,128]{2,1,0:T(8,128)} %scan_back.1), channel_id=1, replica_groups=mesh['sp_0'=4,'sp_1'=4,'sp_2'=2,'tp'=4] {'sp_0','sp_1','sp_2'}, dimensions={0} | all-to-all | bytes 1835008 | tf_op jit(solution)/shard_map/all_to_all | solution.py:276
  84.0 4.7 %finish.1 = (f32[128,1024]{1,0:T(8,128)}, f32[32,256]{1,0:T(8,128)}, f32[2,256]{1,0:T(2,128)}) custom-call(bf16[128,256]{1,0:T(8,128)(2,1)} %get-tuple-element.22.f_ref, bf16[128,256]{1,0:T(8,128)(2,1)} %get-tuple-element.23.b_ref, bf16[128,256]{1,0:T(8,128)(2,1)} %get-tuple-element.24.v_ref, f32[128,256]{1,0:T(8,128)} %get-tuple-element.25.cf_ref, ...), custom_call_target="tpu_custom_call" | custom-call | tf_op jit(solution)/shard_map/finish/pallas_call | solution.py:299
  88.7 14.2 %all_to_all.31 = f32[4,32,1024]{2,1,0:T(8,128)S(1)} all-to-all(f32[4,32,1024]{2,1,0:T(8,128)} %bitcast.5), channel_id=1, replica_groups=mesh['sp_0'=4,'sp_1'=4,'sp_2'=2,'tp'=4] {'tp'}, dimensions={0} | all-to-all | bytes 1048576 | tf_op jit(solution)/shard_map/all_to_all | solution.py:276
  102.9 0.7 fusion.1
Async XLA Ops:
  24.6 12.8 %all-to-all-start.1 = ((f32[32,16,128]{2,1,0:T(8,128)}), f32[32,16,128]{2,1,0:T(8,128)S(1)}, u32[]{:S(2)}, u32[]{:S(2)}) async-start(f32[32,16,128]{2,1,0:T(8,128)} %scan.1), calls=%async_computation.1 | async-start | bytes 524288 | tf_op jit(solution)/shard_map/all_to_all | solution.py:276
  37.4 0.7 copy-start.1
  43.2 3.9 %copy-start.3 = (f32[32,32,128]{2,1,0:T(8,128)S(1)}, f32[32,32,128]{2,1,0:T(8,128)}, u32[]{:S(2)}) copy-start(f32[32,32,128]{2,1,0:T(8,128)} %get-tuple-element.31) | copy-start | bytes 1572868
  43.2 17.1 %all-to-all-start.2 = ((f32[32,40,128]{2,1,0:T(8,128)}), f32[32,40,128]{2,1,0:T(8,128)S(1)}, u32[]{:S(2)}, u32[]{:S(2)}) async-start(f32[32,40,128]{2,1,0:T(8,128)} %get-tuple-element.29), calls=%async_computation.2 | async-start | bytes 1310720 | tf_op jit(solution)/shard_map/all_to_all | solution.py:276
  47.1 2.0 %collective-permute-start = (f32[32,32,128]{2,1,0:T(8,128)S(1)}, f32[32,32,128]{2,1,0:T(8,128)S(1)}, u32[]{:S(2)}, u32[]{:S(2)}) collective-permute-start(f32[32,32,128]{2,1,0:T(8,128)S(1)} %copy-done.3), channel_id=1, source_target_pairs={{0,4},{4,0},{1,5},{5,1},{2,6},{6,2},{3,7},{7,3},{8,12},{12,8},{9,1... | collective-permute-start | bytes 1572872 | tf_op jit(solution)/shard_map/ppermute | solution.py:294
  49.1 11.2 %copy-start.2 = (f32[32,32,128]{2,1,0:T(8,128)}, f32[32,32,128]{2,1,0:T(8,128)S(1)}, u32[]{:S(2)}) copy-start(f32[32,32,128]{2,1,0:T(8,128)S(1)} %collective-permute-done.other_ref) | copy-start | bytes 1572868
  60.3 0.8 copy-start

commit v2 on v1

v2 whole, which is shorter than its diff:
```python
import jax
import jax.numpy as jnp
from jax import lax
from jax.experimental import pallas as pl
from jax.experimental.pallas import tpu as pltpu
from jax.sharding import Mesh
from jax.sharding import PartitionSpec as P

SP = ("sp_0", "sp_1", "sp_2")
SP_TP = ("sp_0", "sp_1", "sp_2", "tp")
N = 32
T = 128
K = 128
HEADS = 2
W = HEADS * K
D = 1024
TOKENS = 4096.0
Q_SCALE = K ** (-0.5)
OUT_SCALE = TOKENS ** (-0.5)
NORM_EPS = 1e-06
F32 = jnp.float32
BF16 = jnp.bfloat16
NN = ((1,), (0,))
NT = ((1,), (1,))
VMEM = pl.BlockSpec(memory_space=pltpu.VMEM)
SMEM = pl.BlockSpec(memory_space=pltpu.SMEM)
VMEM_LIMIT = 16 << 20
MANY, FEW = 400_000_000, 10_000_000


def dot(a, b, dims):
    return lax.dot_general(a, b, (dims, ((), ())), preferred_element_type=F32)


def split(a):
    high = a.astype(BF16)
    return high, (a - high.astype(F32)).astype(BF16)


def dot3(a, b, dims):
    (ah, al), (bh, bl) = split(a), split(b)
    return dot(ah, bh, dims) + (dot(ah, bl, dims) + dot(al, bh, dims))


def dot2(a, b, dims):
    bh, bl = split(b)
    return dot(a, bh, dims) + dot(a, bl, dims)


def dot2r(a, b, dims):
    ah, al = split(a)
    return dot(ah, b, dims) + dot(al, b, dims)


def lower_triangle():
    row = lax.broadcasted_iota(jnp.int32, (T, T), 0)
    col = lax.broadcasted_iota(jnp.int32, (T, T), 1)
    return row >= col, row <= col


def opening_of(rate):
    r = rate * (1.0 / TOKENS)
    return r * (1.0 - r * (1 / 2) * (1.0 - r * (1 / 3) * (1.0 - r * (1 / 4))))


def gates(raw, opening):
    x = raw.astype(F32)
    closed = 1.0 / (1.0 + jnp.exp(x))
    return closed, opening * closed


def log_forget_of(key):
    return -key * (1.0 + key * (1 / 2 + key * (1 / 3 + key * (1 / 4 + key * (1 / 5)))))


def project_kernel(x_ref, wf_ref, wb_ref, wv_ref, rate_ref, f_ref, b_ref, v_ref, cf_ref, cb_ref, msg_ref):
    x = x_ref[...]
    low, up = lower_triangle()
    low, up = low.astype(BF16), up.astype(BF16)
    v = dot(x, wv_ref[...], NN).astype(BF16)
    v_ref[...] = v
    opening = opening_of(rate_ref[...])
    decayed = []
    for d, (w_ref, raw_ref, cum_ref, tri) in enumerate(((wf_ref, f_ref, cf_ref, low), (wb_ref, b_ref, cb_ref, up))):
        raw = dot(x, w_ref[...], NN).astype(BF16)
        raw_ref[...] = raw
        _, key = gates(raw, opening[d : d + 1])
        cum = dot2(tri, log_forget_of(key), NN)
        cum_ref[...] = cum
        last = cum[T - 1 : T] if d == 0 else cum[0:1]
        decayed.append((jnp.exp(last), key * jnp.exp(last - cum)))
    for h in range(HEADS):
        cols = slice(h * K, (h + 1) * K)
        v_t = v[:, cols].astype(F32).T.astype(BF16)
        group = slice(h * 16, (h + 1) * 16)
        msg_ref[group, 16:24, :] = jnp.zeros((16, 8, K), F32)
        both = dot2(v_t, jnp.concatenate([left[:, cols] for _, left in decayed], axis=1), NN)
        for d, (all_keep, left) in enumerate(decayed):
            msg_ref[group, 8 * d : 8 * d + 8, :] = both[:, d * K : (d + 1) * K].reshape(16, 8, K)
            msg_ref[group, 16 + d : 17 + d, :] = jnp.broadcast_to(all_keep[:, cols].reshape(1, 1, K), (16, 1, K))


def local_kernel(
    x_ref, wq_ref, f_ref, b_ref, v_ref, cf_ref, cb_ref, rate_ref,
    a_ref, bk_ref, scores_ref, inner_ref, reach_ref, tail_ref, share_ref,
):
    low, up = lower_triangle()
    opening = opening_of(rate_ref[...])
    query = dot(x_ref[...], wq_ref[...], NN).astype(BF16).astype(F32) * Q_SCALE
    for h in range(HEADS):
        cols = slice(h * K, (h + 1) * K)
        v = v_ref[:, cols]
        v_t = v.astype(F32).T.astype(BF16)
        scores = jnp.zeros((T, T), F32)
        zs = []
        for d, (raw_ref, cum_ref, tri) in enumerate(((f_ref, cf_ref, low), (b_ref, cb_ref, up))):
            closed, key = gates(raw_ref[:, cols], opening[d : d + 1, cols])
            cum = cum_ref[:, cols]
            fade = jnp.exp(-cum)
            last = cum[T - 1 : T] if d == 0 else cum[0:1]
            a = query[:, cols] * jnp.exp(cum)
            b = key * fade
            both = slice((2 * h + d) * K, (2 * h + d + 1) * K)
            a_ref[:, both] = a
            bk_ref[:, both] = b
            scores = scores + jnp.where(tri, dot3(a, b, NT), 0.0)
            share = closed / (1.0 - key)
            before = dot2(tri.astype(BF16), share, NN)
            share_ref[:, both] = before
            total = before[T - 1 : T] if d == 0 else before[0:1]
            keep = jnp.exp(last)
            zs.append(keep * fade * (closed - (total - before) * key))
            tail_ref[2 * h + d : 2 * h + d + 1, :] = keep * total
        scores_ref[:, cols] = scores
        inner_ref[:, cols] = dot2r(scores, v, NN)
        reach_ref[:, 2 * h * K : 2 * (h + 1) * K] = dot2(v_t, jnp.concatenate(zs, axis=1), NN)


def scan_kernel(got_ref, out_ref):
    run_f = run_b = jnp.zeros((8, K), F32)
    for i in range(N):
        j = N - 1 - i
        out_ref[i, 0:8, :] = run_f
        out_ref[j, 8:16, :] = run_b
        run_f = got_ref[i, 16:17, :] * run_f + got_ref[i, 0:8, :]
        run_b = got_ref[j, 17:18, :] * run_b + got_ref[j, 8:16, :]


def states_of(ref, h):
    group = slice(h * 16, (h + 1) * 16)
    return [ref[group, 8 * d : 8 * d + 8, :].reshape(K, K) for d in range(2)]


def mix_kernel(a_ref, inner_ref, reach_ref, tail_ref, gain_ref, cot_ref, in_ref, msg_ref, dm_ref):
    gain = gain_ref[...]
    for h in range(HEADS):
        cols = slice(h * K, (h + 1) * K)
        wide = slice(2 * h * K, 2 * (h + 1) * K)
        group = slice(h * 16, (h + 1) * 16)
        a = a_ref[:, wide]
        states = jnp.concatenate(states_of(in_ref, h), axis=1)
        mixed = inner_ref[:, cols] + dot3(a, states, NT)
        inv = lax.rsqrt(jnp.mean(mixed * mixed, axis=-1, keepdims=True) + NORM_EPS)
        scaled = cot_ref[:, cols].astype(F32) * gain
        d_mixed = inv * scaled - mixed * (inv * inv * inv * jnp.mean(scaled * mixed, axis=-1, keepdims=True))
        dm_ref[:, cols] = d_mixed
        seeds = dot3(d_mixed.T, a, NN)
        tail = jnp.concatenate([tail_ref[2 * h + d : 2 * h + d + 1, :] for d in range(2)], axis=1)
        reach = reach_ref[:, wide] - tail * states
        for d in range(2):
            half = slice(d * K, (d + 1) * K)
            msg_ref[group, 8 * d : 8 * d + 8, :] = seeds[:, half].reshape(16, 8, K)
            msg_ref[group, 16 + 8 * d : 24 + 8 * d, :] = reach[:, half].reshape(16, 8, K)


def query_kernel(
    core_ref, x_ref, cf_ref, cb_ref, v_ref, a_ref, bk_ref, in_ref, dm_ref,
    own_ref, other_ref, gq_ref, local_ref, ada_ref,
):
    low, up = lower_triangle()
    grad_q = []
    for h in range(HEADS):
        cols = slice(h * K, (h + 1) * K)
        d_mixed = dm_ref[:, cols]
        d_scores = dot2r(d_mixed, v_ref[:, cols], NT)
        dq = jnp.zeros((T, K), F32)
        for d, (state, cum_ref, tri) in enumerate(zip(states_of(in_ref, h), (cf_ref, cb_ref), (low, up))):
            both = slice((2 * h + d) * K, (2 * h + d + 1) * K)
            local = jnp.where(tri, d_scores, 0.0)
            local_ref[:, both] = local
            da = dot3(
                jnp.concatenate([local, d_mixed], axis=1), jnp.concatenate([bk_ref[:, both], state], axis=0), NN
            )
            dq = dq + da * jnp.exp(cum_ref[:, cols])
            ada_ref[:, both] = a_ref[:, both] * da
        grad_q.append((dq * Q_SCALE).astype(BF16))
    gq = jnp.concatenate(grad_q, axis=1)
    gq_ref[...] = gq
    term = dot(x_ref[...].astype(F32).T.astype(BF16), gq, NN).reshape(N, 2, 16, W)
    first = core_ref[0] == 0
    own = jnp.where(first, term[:, 0], term[:, 1])
    other = jnp.where(first, term[:, 1], term[:, 0])
    for part, ref in ((own, own_ref), (other, other_ref)):
        for h in range(HEADS):
            ref[:, 16 * h : 16 * h + 16, :] = part[:, :, h * K : (h + 1) * K]


def key_kernel(
    f_ref, b_ref, cf_ref, cb_ref, rate_ref, a_ref, bk_ref, scores_ref, share_ref, local_ref, ada_ref, dm_ref,
    db_ref, dv_ref, floor_ref,
):
    opening = opening_of(rate_ref[...])
    for h in range(HEADS):
        cols = slice(h * K, (h + 1) * K)
        dv_ref[:, cols] = dot3(scores_ref[:, cols].T, dm_ref[:, cols], NN)
        for d, (raw_ref, cum_ref) in enumerate(((f_ref, cf_ref), (b_ref, cb_ref))):
            both = slice((2 * h + d) * K, (2 * h + d + 1) * K)
            db = dot3(local_ref[:, both].T, a_ref[:, both], NN)
            db_ref[:, both] = db
            closed, _ = gates(raw_ref[:, cols], opening[d : d + 1, cols])
            floor = closed * (db * jnp.exp(-cum_ref[:, cols])) - share_ref[:, both] * (
                ada_ref[:, both] - bk_ref[:, both] * db
            )
            floor_ref[2 * h + d : 2 * h + d + 1, :] = jnp.sum(floor, axis=0, keepdims=True)


def scan_back_kernel(keep_ref, got_ref, own_ref, other_ref, local_ref, out_ref):
    run_f = run_b = reach_f = reach_b = jnp.zeros((8, K), F32)
    for i in range(N):
        j = N - 1 - i
        out_ref[j, 0:8, :] = run_f
        out_ref[i, 8:16, :] = run_b
        reach_f = reach_f + run_f * got_ref[j, 16:24, :]
        reach_b = reach_b + run_b * got_ref[i, 24:32, :]
        run_f = keep_ref[j, 16:17, :] * run_f + got_ref[j, 0:8, :]
        run_b = keep_ref[i, 17:18, :] * run_b + got_ref[i, 8:16, :]
    out_ref[:, 16:48, :] = own_ref[...] + other_ref[...]
    tail = [jnp.sum(reach_f, axis=0, keepdims=True), jnp.sum(reach_b, axis=0, keepdims=True)]
    tail = jnp.concatenate(tail + [local_ref[...], jnp.zeros((2, K), F32)], axis=0)
    out_ref[:, 48:56, :] = jnp.broadcast_to(tail[None], (N, 8, K))


def first_term_kernel(gq_ref, wq_ref, term_ref):
    term_ref[...] = dot(gq_ref[...], wq_ref[...], NT)


def finish_kernel(
    f_ref, b_ref, v_ref, cf_ref, cb_ref, rate_ref, in_ref, got_ref,
    bk_ref, db_ref, dv_ref, ada_ref, first_ref, wf_ref, wb_ref, wv_ref,
    term_ref, weight_ref, floor_ref,
):
    low, up = lower_triangle()
    rate = rate_ref[...]
    opening = opening_of(rate)
    g_raw = ([], [])
    g_value = []
    rows = got_ref[:, 48:56, :]
    local_floor = jnp.sum(rows, axis=0)
    floors = ([], [])
    for h in range(HEADS):
        cols = slice(h * K, (h + 1) * K)
        wide = slice(2 * h * K, 2 * (h + 1) * K)
        flows = states_of(got_ref, h)
        flow = jnp.concatenate(flows, axis=1)
        states = states_of(in_ref, h)
        d_lefts = dot2(v_ref[:, cols], flow, NN)
        owned = jnp.sum(rows[h * 16 : (h + 1) * 16], axis=0)
        lefts = []
        for d, (raw_ref, cum_ref, rev) in enumerate(((f_ref, cf_ref, up), (b_ref, cb_ref, low))):
            both = slice((2 * h + d) * K, (2 * h + d + 1) * K)
            closed, key = gates(raw_ref[:, cols], opening[d : d + 1, cols])
            opened = 1.0 / (1.0 + jnp.exp(-raw_ref[:, cols].astype(F32)))
            cum = cum_ref[:, cols]
            last = cum[T - 1 : T] if d == 0 else cum[0:1]
            keep = jnp.exp(last)
            b = bk_ref[:, both]
            left = b * keep
            lefts.append(left)
            d_left = d_lefts[:, d * K : (d + 1) * K]
            db = db_ref[:, both] + keep * d_left
            dc = ada_ref[:, both] - b * db
            total = jnp.sum(left * d_left, axis=0, keepdims=True)
            total = total + keep * jnp.sum(states[d] * flows[d], axis=0, keepdims=True)
            d_log = dot2(rev.astype(BF16), dc, NN) + total
            whole = db * jnp.exp(-cum) - d_log / (1.0 - key)
            g_raw[d].append((-key * opened * whole).astype(BF16))
            floors[d].append(owned[d : d + 1] + local_floor[2 + 2 * h + d : 3 + 2 * h + d])
        dv = dv_ref[:, cols] + dot3(jnp.concatenate(lefts, axis=1), flow, NT)
        g_value.append(dv.astype(BF16))
    out = first_ref[...] + dot(jnp.concatenate(g_raw[0], axis=1), wf_ref[...], NT)
    out = out + dot(jnp.concatenate(g_raw[1], axis=1), wb_ref[...], NT)
    out = out + dot(jnp.concatenate(g_value, axis=1), wv_ref[...], NT)
    term_ref[...] = out
    for c in range(2):
        acc = got_ref[c, 16:48, :]
        for j in range(1, N // 2):
            acc = acc + got_ref[2 * j + c, 16:48, :]
        for h in range(HEADS):
            weight_ref[16 * c : 16 * c + 16, h * K : (h + 1) * K] = acc[16 * h : 16 * h + 16] * OUT_SCALE
    shift = jnp.exp(rate * (-1.0 / TOKENS)) * (OUT_SCALE / TOKENS)
    for d in range(2):
        floor_ref[d : d + 1, :] = jnp.concatenate(floors[d], axis=1) * shift[d : d + 1]


def shape(*dims, dtype=F32):
    return jax.ShapeDtypeStruct(dims, dtype)


def call(kernel, out_shape, specs, name, flops):
    many = isinstance(out_shape, (tuple, list))
    return pl.pallas_call(
        kernel,
        out_shape=out_shape,
        in_specs=specs,
        out_specs=[VMEM] * len(out_shape) if many else VMEM,
        name=name,
        cost_estimate=pl.CostEstimate(flops=flops, bytes_accessed=1 << 20, transcendentals=0),
        compiler_params=pltpu.CompilerParams(vmem_limit_bytes=VMEM_LIMIT),
    )


def exchange(array, axes):
    return lax.all_to_all(array, axes, 0, 0, tiled=True)


def body(x, w_query, w_forget_fwd, w_forget_bwd, w_value, floor_rate, gain, cotangent):
    tok, wide = shape(T, W), shape(T, 2 * W)
    tok16 = shape(T, W, dtype=BF16)
    f, b, v, cf, cb, sums = call(
        project_kernel, (tok16, tok16, tok16, tok, tok, shape(N, 24, K)), [VMEM] * 5, "project", MANY
    )(x, w_forget_fwd, w_forget_bwd, w_value, floor_rate)
    sums = exchange(sums, SP)
    a, bk, scores, inner, reach, tail, share = call(
        local_kernel, (wide, wide, tok, tok, wide, shape(4, K), wide), [VMEM] * 8, "local", MANY
    )(x, w_query, f, b, v, cf, cb, floor_rate)
    inflow = exchange(call(scan_kernel, shape(N, 16, K), [VMEM], "scan", FEW)(sums), SP)
    seeds, dm = call(mix_kernel, (shape(N, 32, K), tok), [VMEM] * 7, "mix", MANY)(
        a, inner, reach, tail, gain.reshape(1, K), cotangent, inflow
    )
    seeds = exchange(seeds, SP)
    core = lax.axis_index("sp_2").reshape(1).astype(jnp.int32)
    own, other, gq, local, ada = call(
        query_kernel, (shape(N, 32, K), shape(N, 32, K), tok16, wide, wide), [SMEM] + [VMEM] * 8, "query", MANY
    )(core, x, cf, cb, v, a, bk, inflow, dm)
    other = lax.ppermute(other, "sp_2", [(0, 1), (1, 0)])
    db, dv, floor = call(key_kernel, (wide, tok, shape(4, K)), [VMEM] * 12, "key", MANY)(
        f, b, cf, cb, floor_rate, a, bk, scores, share, local, ada, dm
    )
    outflow = exchange(
        call(scan_back_kernel, shape(N, 56, K), [VMEM] * 5, "scan_back", FEW)(sums, seeds, own, other, floor), SP
    )
    first = call(first_term_kernel, shape(T, D), [VMEM] * 2, "first_term", MANY)(gq, w_query)
    term, grad_weight, grad_floor = call(
        finish_kernel, (shape(T, D), shape(N, W), shape(2, W)), [VMEM] * 16, "finish", MANY
    )(
        f, b, v, cf, cb, floor_rate, inflow, outflow, bk, db, dv, ada, first, w_forget_fwd, w_forget_bwd, w_value
    )
    pieces = exchange(term, "tp").reshape(4, T // 4, D)
    grad_input = (pieces[0] + pieces[1] + pieces[2] + pieces[3]).astype(BF16)
    return grad_input, grad_weight, grad_floor


def solution(mesh):
    finer = Mesh(mesh.devices.reshape(4, 4, 2, mesh.shape["tp"]), ("sp_0", "sp_1", "sp_2", "tp"))
    return jax.shard_map(
        body,
        mesh=finer,
        in_specs=(
            P(SP, None),
            P(None, "tp"),
            P(None, "tp"),
            P(None, "tp"),
            P(None, "tp"),
            P(None, "tp"),
            P(),
            P(SP, "tp"),
        ),
        out_specs=(P(SP_TP, None), P(SP, "tp"), P(None, "tp")),
        check_vma=False,
    )
```

time: 104 us -> 104 us (level)
  blocking collectives: 53.4 us -> 32.6 us
  local copies, waits for them, and re-layouts: 1.53 us -> 20.3 us
  Pallas kernels: 17.4 us -> 8.94 us
  waiting for transfers between devices: 21.8 us -> 27.3 us
  starting transfers between devices: 8.07 us -> 12 us
    all_to_all x3 -> x2, blocking collectives: 53.4 us -> 32.6 us  [exchange(): return lax.all_to_all(array, axes, 0, 0, tiled=True)]
    unnamed x8 -> x70, local copies, waits for them, and re-layouts: 1.53 us -> 20.3 us
    pallas_call x5 -> x9, Pallas kernels: 17.4 us -> 8.94 us  [the longest x1 1.83 us: body(): call(finish_kernel, (shape(T, D), shape(N, W), shape(2, W)), [VMEM] * 16,...]
    all_to_all x2 -> x3, waiting for transfers between devices: 20.2 us -> 27.3 us  [exchange(): return lax.all_to_all(array, axes, 0, 0, tiled=True)]
    all_to_all x2 -> x3, starting transfers between devices: 7.7 us -> 11.9 us  [exchange(): return lax.all_to_all(array, axes, 0, 0, tiled=True)]
    ppermute x1, waiting for transfers between devices: 1.62 us -> 0.01 us  [body(): other = lax.ppermute(other, 'sp_2', [(0, 1), (1, 0)])]
  transfers between devices with their start and end apart: 3 -> 4, of which waited for: 3 -> 3; matrix products, arithmetic and copies ran while one was open for 0% -> 0% of each run, Pallas kernels for 0% -> 2%
where the time goes in v2:
time: 104 us; the launch traced here: 103 us
  blocking collectives  32.6 us (31%)
  waiting for transfers between devices  27.3 us (26%)
  local copies, waits for them, and re-layouts  20.3 us (20%)
  starting transfers between devices  12 us (12%)
  Pallas kernels  8.94 us (9%)
    all_to_all x2, blocking collectives, exchange(): return lax.all_to_all(array, axes, 0, 0, tiled=True)  32.6 us
    all_to_all x3, waiting for transfers between devices, exchange(): return lax.all_to_all(array, axes, 0, 0, tiled=True)  27.3 us
    unnamed x70, local copies, waits for them, and re-layouts  20.3 us
    all_to_all x3, starting transfers between devices, exchange(): return lax.all_to_all(array, axes, 0, 0, tiled=True)  11.9 us
  transfers between devices with their start and end apart: 4, of which 3 were waited for; matrix products, arithmetic and copies ran while one was open for 0% of the time, Pallas kernels for 2%

profile of v2, /device:TPU:1, one launch (start us, length us, event | category | flops | bytes accessed | tf_op | source)
XLA Modules:
  0.0 102.7 jit_solution(7354943338593499407)
XLA Ops:
  0.6 0.0 copy-start
  0.6 1.0 %copy-done = bf16[1024,256]{1,0:T(8,128)(2,1)S(1)} copy-done((bf16[1024,256]{1,0:T(8,128)(2,1)S(1)}, bf16[1024,256]{1,0:T(8,128)(2,1)}, u32[]{:S(2)}) %copy-start) | copy-done | bytes 524312
  1.7 1.0 %copy-done.2 = bf16[1024,256]{1,0:T(8,128)(2,1)S(1)} copy-done((bf16[1024,256]{1,0:T(8,128)(2,1)S(1)}, bf16[1024,256]{1,0:T(8,128)(2,1)}, u32[]{:S(2)}) %copy-start.2) | copy-done | bytes 524312
  2.7 1.0 %copy-done.4 = bf16[1024,256]{1,0:T(8,128)(2,1)S(1)} copy-done((bf16[1024,256]{1,0:T(8,128)(2,1)S(1)}, bf16[1024,256]{1,0:T(8,128)(2,1)}, u32[]{:S(2)}) %copy-start.4) | copy-done | bytes 524312
  3.8 0.9 copy-done.6
  4.7 0.7 copy-done.27
  5.4 0.9 project.1
  6.3 0.0 copy-start.11
  6.3 18.5 %all_to_all.29.got_ref.keep_ref = f32[32,24,128]{2,1,0:T(8,128)S(1)} all-to-all(f32[32,24,128]{2,1,0:T(8,128)S(1)} %get-tuple-element.34), channel_id=1, replica_groups=mesh['sp_0'=4,'sp_1'=4,'sp_2'=2,'tp'=4] {'sp_0','sp_1','sp_2'}, dimensions={0} | all-to-all | bytes 786432 | tf_op jit(solution)/shard_map/all_to_all | solution.py:323
  24.9 0.8 scan.1
  25.6 3.9 %all-to-all-start.1 = ((f32[32,16,128]{2,1,0:T(8,128)}), f32[32,16,128]{2,1,0:T(8,128)S(1)}, u32[]{:S(2)}, u32[]{:S(2)}) async-start(f32[32,16,128]{2,1,0:T(8,128)} %scan.1), calls=%async_computation.1 | async-start | bytes 524288 | tf_op jit(solution)/shard_map/all_to_all | solution.py:323
  29.6 0.0 copy-start.31
  29.6 1.1 %local.1 = (f32[128,512]{1,0:T(8,128)S(1)}, f32[128,512]{1,0:T(8,128)S(1)}, f32[128,256]{1,0:T(8,128)S(1)}, f32[128,256]{1,0:T(8,128)S(1)}, f32[128,512]{1,0:T(8...) custom-call(bf16[128,1024]{1,0:T(8,128)(2,1)S(1)} %copy-done.7, bf16[1024,256]{1,0:T(8,128)(2,1)S(1)} %copy-done.29, ...), custom_call_target="tpu_custom_call" | custom-call | flops 400000000 | bytes 1048576 | tf_op jit(solution)/shard_map/local/pallas_call | solution.py:333
  30.7 0.7 copy-done.19
  31.4 7.1 %all-to-all-done.1.in_ref = f32[32,16,128]{2,1,0:T(8,128)S(1)} async-done(((f32[32,16,128]{2,1,0:T(8,128)}), f32[32,16,128]{2,1,0:T(8,128)S(1)}, u32[]{:S(2)}, u32[]{:S(2)}) %all-to-all-start.1) | async-done | bytes 262176 | tf_op jit(solution)/shard_map/all_to_all | solution.py:323
  38.6 0.7 copy-done.34
  39.2 0.7 mix.1
  40.0 1.8 %query.1 = (f32[32,32,128]{2,1,0:T(8,128)S(1)}, f32[32,32,128]{2,1,0:T(8,128)}, bf16[128,256]{1,0:T(8,128)(2,1)S(1)}, f32[128,512]{1,0:T(8,128)S(1)}, f32[128,512]{1,0:T(8,128)S(1)}) custom-call(s32[1]{0:T(128)} %bitcast.1.core_ref, bf16[128,1024]{1,0:T(8,128)(2,1)S(1)} %copy-done.7, f32[128,256]{1,0:T(8,128)S(1)} %get-tuple-element.32.cf_ref, ...), custom_call_target="tpu_custom_call" | custom-call | flops 400000000 | bytes 1048576 | tf_op jit(solution)/shard_map/query/pallas_call | solution.py:342
  41.8 0.7 copy-done.21
  42.5 0.6 copy-done.32
  43.1 0.1 collective-permute-start
  43.3 3.9 %all-to-all-start.2 = ((f32[32,32,128]{2,1,0:T(8,128)}), f32[32,32,128]{2,1,0:T(8,128)S(1)}, u32[]{:S(2)}, u32[]{:S(2)}) async-start(f32[32,32,128]{2,1,0:T(8,128)} %copy-done.8), calls=%async_computation.2 | async-start | bytes 1048576 | tf_op jit(solution)/shard_map/all_to_all | solution.py:323
  47.2 0.0 copy-start.28
  47.2 0.7 copy-done.28
  47.9 0.9 copy-done.20
  48.8 0.9 copy-done.22
  49.8 0.9 copy-done.26
  50.7 0.4 key.1
  51.1 0.7 copy-done.17
  51.8 0.7 copy-done.23
  52.5 6.5 %all-to-all-done.2.got_ref = f32[32,32,128]{2,1,0:T(8,128)S(1)} async-done(((f32[32,32,128]{2,1,0:T(8,128)}), f32[32,32,128]{2,1,0:T(8,128)S(1)}, u32[]{:S(2)}, u32[]{:S(2)}) %all-to-all-start.2) | async-done | bytes 524320 | tf_op jit(solution)/shard_map/all_to_all | solution.py:323
  58.9 1.1 %scan_back.1 = f32[32,56,128]{2,1,0:T(8,128)} custom-call(f32[32,24,128]{2,1,0:T(8,128)S(1)} %all_to_all.29.got_ref.keep_ref, f32[32,32,128]{2,1,0:T(8,128)S(1)} %all-to-all-done.2.got_ref, f32[32,32,128]{2,1,0:T(8,128)S(1)} %get-tuple-element.42.own_ref, f32[32,32,128]{2,1,0:T(8,128)S(1)} %collective-permute-done.other_ref, ...), custom_call_target="tpu_custom_call" | custom-call | flops 10000000 | bytes 1048576 | tf_op jit(solution)/shard_map/scan_back/pallas_call | solution.py:350
  60.0 4.0 %all-to-all-start.3 = ((f32[32,56,128]{2,1,0:T(8,128)}), f32[32,56,128]{2,1,0:T(8,128)S(1)}, u32[]{:S(2)}, u32[]{:S(2)}) async-start(f32[32,56,128]{2,1,0:T(8,128)} %scan_back.1), calls=%async_computation.3 | async-start | bytes 1835008 | tf_op jit(solution)/shard_map/all_to_all | solution.py:323
  64.1 0.0 copy-start.30
  64.1 1.0 %copy-done.30 = bf16[1024,256]{1,0:T(8,128)(2,1)S(1)} copy-done((bf16[1024,256]{1,0:T(8,128)(2,1)S(1)}, bf16[1024,256]{1,0:T(8,128)(2,1)}, u32[]{:S(2)}) %copy-start.30) | copy-done | bytes 524312
  65.1 0.8 copy-done.33
  65.9 0.3 first_term.1.first_ref
  66.3 0.8 copy-done.9
  67.1 13.7 %all-to-all-done.3.got_ref = f32[32,56,128]{2,1,0:T(8,128)S(1)} async-done(((f32[32,56,128]{2,1,0:T(8,128)}), f32[32,56,128]{2,1,0:T(8,128)S(1)}, u32[]{:S(2)}, u32[]{:S(2)}) %all-to-all-start.3) | async-done | bytes 917536 | tf_op jit(solution)/shard_map/all_to_all | solution.py:323
  80.8 1.0 %copy-done.10 = f32[128,1024]{1,0:T(8,128)S(1)} copy-done((f32[128,1024]{1,0:T(8,128)S(1)}, f32[128,1024]{1,0:T(8,128)}, u32[]{:S(2)}) %copy-start.10) | copy-done | bytes 524312
  81.8 0.8 copy-done.12
  82.6 0.8 copy-done.14
  83.5 0.8 copy-done.16
  84.3 0.9 copy-done.18
  85.3 0.9 copy-done.24
  86.2 1.8 %finish.1 = (f32[128,1024]{1,0:T(8,128)S(1)}, f32[32,256]{1,0:T(8,128)}, f32[2,256]{1,0:T(2,128)}) custom-call(bf16[128,256]{1,0:T(8,128)(2,1)S(1)} %copy-done.12, bf16[128,256]{1,0:T(8,128)(2,1)S(1)} %copy-done.14, bf16[128,256]{1,0:T(8,128)(2,1)S(1)} %copy-done.16, f32[128,256]{1,0:T(8,128)S(1)} %get-tuple-element.32.cf_ref, ...), custom_call_target="tpu_custom_call" | custom-call | flops 400000000 | bytes 1048576 | tf_op jit(solution)/shard_map/finish/pallas_call | solution.py:353
  88.0 14.1 %all_to_all.30 = f32[4,32,1024]{2,1,0:T(8,128)S(1)} all-to-all(f32[4,32,1024]{2,1,0:T(8,128)S(1)} %bitcast.5), channel_id=1, replica_groups=mesh['sp_0'=4,'sp_1'=4,'sp_2'=2,'tp'=4] {'tp'}, dimensions={0} | all-to-all | bytes 1048576 | tf_op jit(solution)/shard_map/all_to_all | solution.py:323
  102.1 0.7 fusion.1
  (42 shorter events, 0.1 us)
Async XLA Ops:
  0.6 1.0 %copy-start = (bf16[1024,256]{1,0:T(8,128)(2,1)S(1)}, bf16[1024,256]{1,0:T(8,128)(2,1)}, u32[]{:S(2)}) copy-start(bf16[1024,256]{1,0:T(8,128)(2,1)} %wf_ref.3) | copy-start | bytes 1572868
  1.7 1.0 %copy-start.2 = (bf16[1024,256]{1,0:T(8,128)(2,1)S(1)}, bf16[1024,256]{1,0:T(8,128)(2,1)}, u32[]{:S(2)}) copy-start(bf16[1024,256]{1,0:T(8,128)(2,1)} %wb_ref.3) | copy-start | bytes 1572868
  2.7 1.0 %copy-start.4 = (bf16[1024,256]{1,0:T(8,128)(2,1)S(1)}, bf16[1024,256]{1,0:T(8,128)(2,1)}, u32[]{:S(2)}) copy-start(bf16[1024,256]{1,0:T(8,128)(2,1)} %wv_ref.3) | copy-start | bytes 1572868
  3.8 0.9 copy-start.6
  4.7 0.7 copy-start.27
  6.3 33.7 %copy-start.15 = (bf16[128,256]{1,0:T(8,128)(2,1)}, bf16[128,256]{1,0:T(8,128)(2,1)S(1)}, u32[]{:S(2)}) copy-start(bf16[128,256]{1,0:T(8,128)(2,1)S(1)} %get-tuple-element.31.v_ref) | copy-start | bytes 196612
  6.3 40.9 %copy-start.11 = (bf16[128,256]{1,0:T(8,128)(2,1)}, bf16[128,256]{1,0:T(8,128)(2,1)S(1)}, u32[]{:S(2)}) copy-start(bf16[128,256]{1,0:T(8,128)(2,1)S(1)} %get-tuple-element.29.f_ref) | copy-start | bytes 196612
  6.3 40.9 %copy-start.13 = (bf16[128,256]{1,0:T(8,128)(2,1)}, bf16[128,256]{1,0:T(8,128)(2,1)S(1)}, u32[]{:S(2)}) copy-start(bf16[128,256]{1,0:T(8,128)(2,1)S(1)} %get-tuple-element.30.b_ref) | copy-start | bytes 196612
  24.9 4.7 %copy-start.29 = (bf16[1024,256]{1,0:T(8,128)(2,1)S(1)}, bf16[1024,256]{1,0:T(8,128)(2,1)}, u32[]{:S(2)}) copy-start(bf16[1024,256]{1,0:T(8,128)(2,1)} %wq_ref.3) | copy-start | bytes 1572868
  25.6 4.0 %copy-start.7 = (bf16[128,1024]{1,0:T(8,128)(2,1)S(1)}, bf16[128,1024]{1,0:T(8,128)(2,1)}, u32[]{:S(2)}) copy-start(bf16[128,1024]{1,0:T(8,128)(2,1)} %x_ref.5) | copy-start | bytes 786436
  25.6 12.9 %all-to-all-start.1 = ((f32[32,16,128]{2,1,0:T(8,128)}), f32[32,16,128]{2,1,0:T(8,128)S(1)}, u32[]{:S(2)}, u32[]{:S(2)}) async-start(f32[32,16,128]{2,1,0:T(8,128)} %scan.1), calls=%async_computation.1 | async-start | bytes 524288 | tf_op jit(solution)/shard_map/all_to_all | solution.py:323
  29.6 9.0 %copy-start.31 = (bf16[128,256]{1,0:T(8,128)(2,1)S(1)}, bf16[128,256]{1,0:T(8,128)(2,1)}, u32[]{:S(2)}) copy-start(bf16[128,256]{1,0:T(8,128)(2,1)} %cot_ref.1) | copy-start | bytes 196612
  30.7 0.7 copy-start.19
  31.4 8.5 %copy-start.25 = (f32[128,256]{1,0:T(8,128)}, f32[128,256]{1,0:T(8,128)S(1)}, u32[]{:S(2)}) copy-start(f32[128,256]{1,0:T(8,128)S(1)} %get-tuple-element.44.scores_ref) | copy-start | bytes 393220
  38.6 0.7 copy-start.34
  40.0 3.3 %copy-start.8 = (f32[32,32,128]{2,1,0:T(8,128)}, f32[32,32,128]{2,1,0:T(8,128)S(1)}, u32[]{:S(2)}) copy-start(f32[32,32,128]{2,1,0:T(8,128)S(1)} %get-tuple-element.39) | copy-start | bytes 1572868
  41.8 0.7 copy-start.21
  42.5 0.6 copy-start.32
  43.1 15.8 %collective-permute-start = (f32[32,32,128]{2,1,0:T(8,128)}, f32[32,32,128]{2,1,0:T(8,128)S(1)}, u32[]{:S(2)}, u32[]{:S(2)}) collective-permute-start(f32[32,32,128]{2,1,0:T(8,128)} %get-tuple-element.43), channel_id=1, source_target_pairs={{0,4},{4,0},{1,5},{5,1},{2,6},{6,2},{3,7},{7,3},{8,12},{12,8},{9,1... | collective-permute-start | bytes 1572872 | tf_op jit(solution)/shard_map/ppermute | solution.py:345
  43.3 15.7 %all-to-all-start.2 = ((f32[32,32,128]{2,1,0:T(8,128)}), f32[32,32,128]{2,1,0:T(8,128)S(1)}, u32[]{:S(2)}, u32[]{:S(2)}) async-start(f32[32,32,128]{2,1,0:T(8,128)} %copy-done.8), calls=%async_computation.2 | async-start | bytes 1048576 | tf_op jit(solution)/shard_map/all_to_all | solution.py:323
  47.2 0.7 copy-start.28
  47.9 0.9 copy-start.20
  48.8 0.9 copy-start.22
  49.8 0.9 copy-start.26
  51.1 0.7 copy-start.17
  51.8 0.7 copy-start.23
  60.0 20.7 %copy-start.5 = (bf16[1024,256]{1,0:T(8,128)(2,1)S(1)}, bf16[1024,256]{1,0:T(8,128)(2,1)}, u32[]{:S(2)}) copy-start(bf16[1024,256]{1,0:T(8,128)(2,1)} %wv_ref.3) | copy-start | bytes 1572868
  60.0 20.7 %all-to-all-start.3 = ((f32[32,56,128]{2,1,0:T(8,128)}), f32[32,56,128]{2,1,0:T(8,128)S(1)}, u32[]{:S(2)}, u32[]{:S(2)}) async-start(f32[32,56,128]{2,1,0:T(8,128)} %scan_back.1), calls=%async_computation.3 | async-start | bytes 1835008 | tf_op jit(solution)/shard_map/all_to_all | solution.py:323
  64.1 1.0 %copy-start.30 = (bf16[1024,256]{1,0:T(8,128)(2,1)S(1)}, bf16[1024,256]{1,0:T(8,128)(2,1)}, u32[]{:S(2)}) copy-start(bf16[1024,256]{1,0:T(8,128)(2,1)} %wq_ref.3) | copy-start | bytes 1572868
  65.1 0.8 copy-start.33
  65.9 14.8 %copy-start.1 = (bf16[1024,256]{1,0:T(8,128)(2,1)S(1)}, bf16[1024,256]{1,0:T(8,128)(2,1)}, u32[]{:S(2)}) copy-start(bf16[1024,256]{1,0:T(8,128)(2,1)} %wf_ref.3) | copy-start | bytes 1572868
  65.9 14.8 %copy-start.3 = (bf16[1024,256]{1,0:T(8,128)(2,1)S(1)}, bf16[1024,256]{1,0:T(8,128)(2,1)}, u32[]{:S(2)}) copy-start(bf16[1024,256]{1,0:T(8,128)(2,1)} %wb_ref.3) | copy-start | bytes 1572868
  66.3 0.8 copy-start.9
  80.7 1.0 %copy-start.10 = (f32[128,1024]{1,0:T(8,128)S(1)}, f32[128,1024]{1,0:T(8,128)}, u32[]{:S(2)}) copy-start(f32[128,1024]{1,0:T(8,128)} %copy-done.9) | copy-start | bytes 1572868
  81.8 0.8 copy-start.12
  82.6 0.8 copy-start.14
  83.5 0.8 copy-start.16
  84.3 0.9 copy-start.18
  85.3 0.9 copy-start.24
